TPU v7x, 32 devices: a whole 2x2x4 slice. The times are simulated.
32 devices in a mesh: tp: 8 (over z, x), dp: 4 (over y, core).
Axes of the slice: x: 2, y: 2, z: 4, core: 2. Of those that a mesh axis runs over, the one named last changes fastest.
Arguments:
- stream: bfloat16 [128, 4096], P(None, 'dp'), may hold values from -12 to 12
- history: int32 [128], P('dp'), may hold values from 1 to 4096, 131072 in all
- input_norm_gain: float32 [2, 4096], P(None, 'dp'), may hold values from 0.1 to 1.9
- query_weight: bfloat16 [2, 4096, 4096], P(None, 'dp', 'tp'), may hold values from -0.09375 to 0.09375
- key_weight: bfloat16 [2, 4096, 4096], P(None, 'dp', 'tp'), may hold values from -0.09375 to 0.09375
- value_weight: bfloat16 [2, 4096, 4096], P(None, 'dp', 'tp'), may hold values from -0.09375 to 0.09375
- gate_weight: bfloat16 [2, 4096, 4096], P(None, 'dp', 'tp'), may hold values from -0.09375 to 0.09375
- adapter_down_weight: bfloat16 [2, 4096, 128], P(None, 'dp'), may hold values from -0.09375 to 0.09375
- decay_up_weight: float32 [2, 64, 4096], P(None, None, 'tp'), may hold values from -3 to 3
- rate_up_weight: float32 [2, 64, 4096], P(None, None, 'tp'), may hold values from -3 to 3
- decay_offset: float32 [2, 4096], P(None, 'tp'), may hold values from -3 to 1
- head_norm_gain: float32 [2, 4096], P(None, 'tp'), may hold values from 0.1 to 1.9
- output_weight: bfloat16 [2, 4096, 4096], P(None, 'tp', 'dp'), may hold values from -0.09375 to 0.09375
- recurrent_state: float32 [2, 128, 64, 4096], P(None, 'dp', 'tp'), may hold values from -5 to 5
Outputs:
- stream_out: bfloat16 [128, 4096], P(None, 'dp')
- state_out: float32 [2, 128, 64, 4096], P(None, 'dp', 'tp')
All inputs are finite; a program needn't handle non-finite values. No bound on the sum of `history` on one device may be relied on, other than what follows from the above.
Results may differ from a plain program's by a relative error of at most 0.024.
Values may be sent and summed in bfloat16 or wider, within the bound.
A program may use at most 128 MiB of HBM per device.

v0:
```python
import functools

import jax
import jax.numpy as jnp
from jax import lax
from jax.experimental import pallas as pl
from jax.experimental.pallas import tpu as pltpu
from jax.sharding import PartitionSpec as P

HEAD = 64
SPAN = 64
BLOCK_COUNT = 2
LANES = 128
NORM_EPS = 0.25
GROUP_EPS = 0.25
DECAY_SCALE = 0.6065306597126334
TILE = 256
PIECES = 2
MESH = pl.DeviceIdType.MESH
F32 = jnp.float32
BF16 = jnp.bfloat16


def sigmoid(z):
    e = jnp.exp(-jnp.abs(z))
    return jnp.where(z >= 0, 1.0, e) / (1.0 + e)


def kernel(
    n_dp,
    n_tp,
    stream_ref,
    history_ref,
    in_gain,
    adapter_hbm,
    key_hbm,
    query_hbm,
    value_hbm,
    gate_hbm,
    decay_up,
    rate_up,
    offset,
    head_gain,
    out_hbm,
    state_hbm,
    stream_out,
    state,
    wa,
    wk,
    wq,
    wv,
    wg,
    wo,
    sent,
    got,
    sq_sent,
    sq_got,
    mixed_all,
    terms,
    terms_got,
    fresh,
    x_ref,
    rows,
    gather1,
    gather2,
    spread,
    load_sem,
    rs_send,
    rs_recv,
    sq_send,
    sq_recv,
    ag_send,
    ag_recv,
    tr_send,
    tr_recv,
    ta_send,
    ta_recv,
):
    me = lax.axis_index("dp")
    lane_me = lax.axis_index("tp")
    batch, depth = stream_ref.shape
    seq = batch // n_dp
    width = wk.shape[2]
    heads = width // HEAD
    count = seq * heads
    part = batch // n_tp
    rank = wa.shape[2] // 2
    vk = state.shape[2]
    tiles = vk // TILE

    loads = {}

    def load(l, i, src, dst):
        loads[l, i] = pltpu.make_async_copy(src.at[l], dst.at[l], load_sem.at[l, i])
        loads[l, i].start()

    def load_all(l):
        load(l, 0, adapter_hbm, wa)
        load(l, 1, key_hbm, wk)
        load(l, 2, query_hbm, wq)
        load(l, 3, value_hbm, wv)
        load(l, 4, gate_hbm, wg)
        load(l, 5, state_hbm, state)
        load(l, 6, out_hbm, wo)

    load_all(0)

    def dp_peer(o):
        return lax.rem(me + o, n_dp)

    def tp_peer(o):
        return lax.rem(lane_me + o, n_tp)

    barrier = pltpu.get_barrier_semaphore()
    for o in range(1, n_dp):
        pl.semaphore_signal(barrier, inc=1, device_id={"dp": dp_peer(o)}, device_id_type=MESH)
    for o in range(1, n_tp):
        pl.semaphore_signal(barrier, inc=1, device_id={"tp": tp_peer(o)}, device_id_type=MESH)

    def fill(t, carry):
        at = pl.ds(pl.multiple_of(t * TILE, TILE), TILE)
        r = (lax.broadcasted_iota(jnp.int32, (TILE, LANES), 0) + t * TILE) // HEAD
        c = lax.broadcasted_iota(jnp.int32, (TILE, LANES), 1)
        gather1[at, :] = jnp.where(r == c, 1.0, 0.0).astype(BF16)
        gather2[at, :] = jnp.where(r + HEAD == c, 1.0, 0.0).astype(BF16)
        r = lax.broadcasted_iota(jnp.int32, (LANES, TILE), 0)
        c = (lax.broadcasted_iota(jnp.int32, (LANES, TILE), 1) + t * TILE) // HEAD
        spread[:, at] = jnp.where((r == c) | (r == c + HEAD), 1.0, 0.0).astype(BF16)
        return carry

    lax.fori_loop(0, tiles, fill, 0)

    low = lax.broadcasted_iota(jnp.int32, (seq, LANES), 1) < HEAD
    low_rows = lax.broadcasted_iota(jnp.int32, (count, LANES), 1) < HEAD

    def to_rows(value, i):
        buf = rows.at[i]
        for j in range(width // LANES):
            pair = value[:, j * LANES : (j + 1) * LANES]
            turned = pltpu.roll(pair, HEAD, 1)
            buf[pl.ds(2 * j, seq, stride=heads), :] = jnp.where(low, pair, turned)
            buf[pl.ds(2 * j + 1, seq, stride=heads), :] = jnp.where(low, turned, pair)
        return rows[i]

    def half_sum(v):
        return jnp.sum(v, axis=1, keepdims=True) * 0.5

    def twice(v):
        return jnp.concatenate([v, v], axis=1)

    x_ref[...] = stream_ref[...].astype(F32)
    spans = jnp.floor(history_ref[...].astype(F32) * (1.0 / SPAN))
    phase = 0.5 + (spans - 3.0 * jnp.floor((spans + 0.5) * (1.0 / 3.0)))
    diagonal = lax.broadcasted_iota(jnp.int32, (seq, seq), 0) == lax.broadcasted_iota(jnp.int32, (seq, seq), 1)
    pos = jnp.sum(jnp.where(diagonal, phase, 0.0), axis=1, keepdims=True)
    mine = pl.ds(pl.multiple_of(me * seq, seq), seq)
    own_part = pl.ds(pl.multiple_of(lane_me * part, part), part)
    sizes = [2 * rank, width, width, width, width]
    starts = [sum(sizes[:c]) for c in range(5)]
    pending = []
    piece = depth // PIECES
    pieces = [slice(p * piece, (p + 1) * piece) for p in range(PIECES)]

    def remote(src, dst, send, recv, where):
        copy = pltpu.make_async_remote_copy(
            src_ref=src, dst_ref=dst, send_sem=send, recv_sem=recv, device_id=where, device_id_type=MESH
        )
        copy.start()
        pending.append(copy)
        return copy

    for l in range(BLOCK_COUNT):
        x = x_ref[...]
        sq_sent[l] = jnp.broadcast_to(jnp.sum(x * x, axis=1, keepdims=True), (batch, LANES))
        scaled = (x * in_gain[l : l + 1, :]).astype(BF16)
        if l == 0:
            pl.semaphore_wait(barrier, n_dp + n_tp - 2)
        sq_copies = []
        for o in range(1, n_dp):
            there = dp_peer(o)
            at = pl.ds(pl.multiple_of(there * seq, seq), seq)
            sq_copies.append(
                remote(sq_sent.at[l, at], sq_got.at[l, o - 1], sq_send.at[l, o - 1], sq_recv.at[l, o - 1], {"dp": there})
            )
        rs_copies = []
        for c, weight in enumerate((wa, wk, wq, wv, wg)):
            loads[l, c].wait()
            cols = pl.ds(starts[c], sizes[c])
            sent[l, :, cols] = jnp.dot(scaled, weight[l], preferred_element_type=F32).astype(BF16)
            for o in range(1, n_dp):
                there = dp_peer(o)
                at = pl.ds(pl.multiple_of(there * seq, seq), seq)
                rs_copies.append(
                    remote(
                        sent.at[l, at, cols],
                        got.at[l, o - 1, :, cols],
                        rs_send.at[l, c, o - 1],
                        rs_recv.at[l, c, o - 1],
                        {"dp": there},
                    )
                )
        if l + 1 < BLOCK_COUNT:
            load_all(l + 1)

        for copy in sq_copies:
            copy.wait_recv()
        squares = sq_sent[l, mine]
        for o in range(1, n_dp):
            squares = squares + sq_got[l, o - 1]
        inv_rms = lax.rsqrt(squares[:, :1] / (depth * n_dp) + NORM_EPS)

        def total(c):
            for copy in rs_copies[c * (n_dp - 1) : (c + 1) * (n_dp - 1)]:
                copy.wait_recv()
            cols = pl.ds(starts[c], sizes[c])
            out = sent[l, mine, cols].astype(F32)
            for o in range(1, n_dp):
                out = out + got[l, o - 1, :, cols].astype(F32)
            return out * inv_rms

        low_rank = total(0)
        z = offset[l : l + 1, :] + jnp.dot(
            jnp.tanh(low_rank[:, :rank]), decay_up[l], precision=lax.Precision.HIGHEST, preferred_element_type=F32
        )
        decay = to_rows(jnp.exp(sigmoid(z) * (-DECAY_SCALE) * pos), 0)
        learn = to_rows(
            sigmoid(
                jnp.dot(low_rank[:, rank:], rate_up[l], precision=lax.Precision.HIGHEST, preferred_element_type=F32)
            ),
            1,
        )
        keys = to_rows(total(1), 2)
        key_unit = keys * lax.rsqrt(half_sum(keys * keys) + 1.0)
        key_rate = key_unit * learn
        rows[1] = key_rate
        query = to_rows(total(2), 3)
        key_query = half_sum(keys * query)
        rate_query = half_sum(key_rate * query)
        unit2 = twice(key_unit)
        query2 = twice(decay * query)
        loads[l, 5].wait()

        def products(t, acc):
            at = pl.ds(pl.multiple_of(t * TILE, TILE), TILE)
            s = state[l, :, at]
            return (
                acc
                + jnp.dot((s * unit2).astype(BF16), gather1[at, :], preferred_element_type=F32)
                + jnp.dot((s * query2).astype(BF16), gather2[at, :], preferred_element_type=F32)
            )

        acc = lax.fori_loop(0, tiles, products, jnp.zeros((count, LANES), F32), unroll=True)
        turned = pltpu.roll(acc, HEAD, 1)
        state_key = jnp.where(low_rows, acc, turned)
        from_state = jnp.where(low_rows, turned, acc)
        value = to_rows(total(3), 4)
        readout = from_state - state_key * rate_query + value * key_query
        mean = half_sum(readout) * (1.0 / HEAD)
        centred = readout - mean
        var = half_sum(centred * centred) * (1.0 / HEAD)
        rows[5] = centred * lax.rsqrt(var + GROUP_EPS)
        gate = sigmoid(total(4)) * head_gain[l : l + 1, :]
        normed = rows.at[5]
        for j in range(width // LANES):
            even = normed[pl.ds(2 * j, seq, stride=heads), :]
            odd = normed[pl.ds(2 * j + 1, seq, stride=heads), :]
            cols = slice(j * LANES, (j + 1) * LANES)
            mixed_all[l, mine, cols] = (jnp.where(low, even, odd) * gate[:, cols]).astype(BF16)
        ag_copies = []
        for o in range(1, n_dp):
            ag_copies.append(
                remote(
                    mixed_all.at[l, mine],
                    mixed_all.at[l, mine],
                    ag_send.at[l, o - 1],
                    ag_recv.at[l, o - 1],
                    {"dp": dp_peer(o)},
                )
            )

        def split(v):
            high = v.astype(BF16)
            rest = (v - high.astype(F32)).astype(BF16)
            return jnp.where(low_rows, high.astype(F32), rest.astype(F32)).astype(BF16)

        value_split = split(value)
        key_split = split(state_key)

        def update(first, last):
            def one(t, carry):
                at = pl.ds(pl.multiple_of(t * TILE, TILE), TILE)
                wide = jnp.dot(value_split, spread[:, at], preferred_element_type=F32)
                drop = jnp.dot(key_split, spread[:, at], preferred_element_type=F32)
                state[l, :, at] = (
                    state[l, :, at] * twice(rows[0]) - drop * twice(rows[1]) + wide * twice(rows[2])
                )
                return carry

            lax.fori_loop(first, last, one, 0, unroll=True)

        cut = [tiles * i // 3 for i in range(4)]
        update(cut[0], cut[1])
        for copy in ag_copies:
            copy.wait_recv()
        loads[l, 6].wait()
        tr_copies = []
        for p in range(PIECES):
            product = jnp.dot(mixed_all[l], wo[l, :, pieces[p]], preferred_element_type=F32)
            terms[l, p] = product.reshape(n_tp, part, piece).astype(BF16)
            for o in range(1, n_tp):
                there = tp_peer(o)
                tr_copies.append(
                    remote(
                        terms.at[l, p, there],
                        terms_got.at[l, p, o - 1],
                        tr_send.at[l, p, o - 1],
                        tr_recv.at[l, p, o - 1],
                        {"tp": there},
                    )
                )
        update(cut[1], cut[2])
        ta_copies = []
        for p in range(PIECES):
            acc = terms[l, p, lane_me].astype(F32)
            for o in range(1, n_tp):
                tr_copies[p * (n_tp - 1) + o - 1].wait_recv()
                acc = acc + terms_got[l, p, o - 1].astype(F32)
            fresh[l, p, lane_me] = (x_ref[own_part, pieces[p]] + acc).astype(BF16)
            for o in range(1, n_tp):
                ta_copies.append(
                    remote(
                        fresh.at[l, p, lane_me],
                        fresh.at[l, p, lane_me],
                        ta_send.at[l, p, o - 1],
                        ta_recv.at[l, p, o - 1],
                        {"tp": tp_peer(o)},
                    )
                )
        update(cut[2], cut[3])
        for copy in ta_copies:
            copy.wait_recv()
        for p in range(PIECES):
            x_ref[:, pieces[p]] = fresh[l, p].astype(F32).reshape(batch, piece)

    stream_out[...] = x_ref[...].astype(BF16)
    for copy in pending:
        copy.wait_send()


def solution(mesh):
    n_dp, n_tp = mesh.shape["dp"], mesh.shape["tp"]

    def body(
        stream,
        history,
        input_norm_gain,
        query_weight,
        key_weight,
        value_weight,
        gate_weight,
        adapter_down_weight,
        decay_up_weight,
        rate_up_weight,
        decay_offset,
        head_norm_gain,
        output_weight,
        recurrent_state,
    ):
        batch, depth = stream.shape
        width = query_weight.shape[2]
        blocks, seq, heads, vk = recurrent_state.shape
        count = seq * heads
        part = batch // n_tp
        columns = 4 * width + adapter_down_weight.shape[2]
        vmem = pl.BlockSpec(memory_space=pltpu.VMEM)
        hbm = pl.BlockSpec(memory_space=pl.ANY)
        dma = pltpu.SemaphoreType.DMA

        def like(w):
            return pltpu.VMEM(w.shape, w.dtype)

        out, new_state = pl.pallas_call(
            functools.partial(kernel, n_dp, n_tp),
            out_shape=(
                jax.ShapeDtypeStruct((batch, depth), BF16),
                pltpu.VMEM((blocks, count, vk), F32),
            ),
            in_specs=[vmem] * 3 + [hbm] * 5 + [vmem] * 4 + [hbm] * 2,
            out_specs=(vmem, vmem),
            scratch_shapes=[
                like(adapter_down_weight),
                like(key_weight),
                like(query_weight),
                like(value_weight),
                like(gate_weight),
                like(output_weight),
                pltpu.VMEM((blocks, batch, columns), BF16),
                pltpu.VMEM((blocks, n_dp - 1, seq, columns), BF16),
                pltpu.VMEM((blocks, batch, LANES), F32),
                pltpu.VMEM((blocks, n_dp - 1, seq, LANES), F32),
                pltpu.VMEM((blocks, batch, width), BF16),
                pltpu.VMEM((blocks, PIECES, n_tp, part, depth // PIECES), BF16),
                pltpu.VMEM((blocks, PIECES, n_tp - 1, part, depth // PIECES), BF16),
                pltpu.VMEM((blocks, PIECES, n_tp, part, depth // PIECES), BF16),
                pltpu.VMEM((batch, depth), F32),
                pltpu.VMEM((6, count, LANES), F32),
                pltpu.VMEM((vk, LANES), BF16),
                pltpu.VMEM((vk, LANES), BF16),
                pltpu.VMEM((LANES, vk), BF16),
                dma((blocks, 7)),
                dma((blocks, 5, n_dp - 1)),
                dma((blocks, 5, n_dp - 1)),
                dma((blocks, n_dp - 1)),
                dma((blocks, n_dp - 1)),
                dma((blocks, n_dp - 1)),
                dma((blocks, n_dp - 1)),
                dma((blocks, PIECES, n_tp - 1)),
                dma((blocks, PIECES, n_tp - 1)),
                dma((blocks, PIECES, n_tp - 1)),
                dma((blocks, PIECES, n_tp - 1)),
            ],
            compiler_params=pltpu.CompilerParams(
                collective_id=0, has_side_effects=True, vmem_limit_bytes=54 * 1024 * 1024
            ),
        )(
            stream,
            history[None, :],
            input_norm_gain,
            adapter_down_weight,
            key_weight,
            query_weight,
            value_weight,
            gate_weight,
            decay_up_weight,
            rate_up_weight,
            decay_offset,
            head_norm_gain,
            output_weight,
            recurrent_state.reshape(blocks, count, vk),
        )
        return out, new_state.reshape(blocks, seq, heads, vk)

    placed = (
        P(None, "dp"),
        P("dp"),
        P(None, "dp"),
        P(None, "dp", "tp"),
        P(None, "dp", "tp"),
        P(None, "dp", "tp"),
        P(None, "dp", "tp"),
        P(None, "dp", None),
        P(None, None, "tp"),
        P(None, None, "tp"),
        P(None, "tp"),
        P(None, "tp"),
        P(None, "tp", "dp"),
        P(None, "dp", "tp", None),
    )
    return jax.shard_map(
        body,
        mesh=mesh,
        in_specs=placed,
        out_specs=(P(None, "dp"), P(None, "dp", "tp", None)),
        check_vma=False,
    )
```

profile of v0, /device:TPU:0, one launch (start us, length us, event | category | flops | bytes accessed | tf_op | source)
XLA Modules:
  0.0 63.7 jit_solution(9263419708692947886)
XLA Ops:
  0.6 58.9 %shard_map.149 = (bf16[128,1024]{1,0:T(8,128)(2,1)}, f32[2,256,4096]{2,1,0:T(8,128)S(1)}) custom-call(bf16[128,1024]{1,0:T(8,128)(2,1)} %stream_ref.1, s32[1,32]{1,0:T(1,128)} %bitcast.5, f32[2,1024]{1,0:T(2,128)} %in_gain.1, bf16[2,1024,128]{2,1,0:T(8,128)(2,1)} %adapter_hbm.1, bf16[2,1024,512]{2,1,0:T(8,128)(2,1)} %key_hbm.1, ...), custom_call_target="tpu_custom_call" | custom-call | tf_op jit(solution)/shard_map/pallas_call | solution.py:382
  59.6 0.0 copy-start
  59.6 3.4 %copy.18 = f32[2,32,8,4096]{3,2,1,0:T(8,128)} copy(f32[2,32,8,4096]{3,2,1,0:T(8,128)S(1)} %bitcast.3) | data formatting | bytes 16777216
  63.0 0.0 copy-done
  63.0 0.7 %copy.19 = bf16[128,1024]{1,0:T(8,128)(2,1)} copy(bf16[128,1024]{1,0:T(8,128)(2,1)S(1)} %copy-done) | data formatting | bytes 524288
Async XLA Ops:
  59.6 3.4 %copy-start = (bf16[128,1024]{1,0:T(8,128)(2,1)S(1)}, bf16[128,1024]{1,0:T(8,128)(2,1)}, u32[]{:S(2)}) copy-start(bf16[128,1024]{1,0:T(8,128)(2,1)} %get-tuple-element.10) | copy-start | bytes 786436
where the time goes:
time: 63.8 us; the launch traced here: 63.7 us
  Pallas kernels  58.9 us (92%)
  local copies, waits for them, and re-layouts  4.11 us (6%)
  between operations  0.65 us (1%)
    pallas_call x1, Pallas kernels, body(): pl.pallas_call(functools.partial(kernel, n_dp, n_tp), out_shape=(jax.Shap...  58.9 us
    unnamed x4, local copies, waits for them, and re-layouts  4.11 us

commit v1 on v0

v1 whole, which is shorter than its diff:
```python
import functools

import jax
import jax.numpy as jnp
from jax import lax
from jax.experimental import pallas as pl
from jax.experimental.pallas import tpu as pltpu
from jax.sharding import PartitionSpec as P

HEAD = 64
SPAN = 64
BLOCK_COUNT = 2
LANES = 128
NORM_EPS = 0.25
GROUP_EPS = 0.25
DECAY_SCALE = 0.6065306597126334
TILE = 256
FLUSHES = 8
MESH = pl.DeviceIdType.MESH
F32 = jnp.float32
BF16 = jnp.bfloat16


def sigmoid(z):
    e = jnp.exp(-jnp.abs(z))
    return jnp.where(z >= 0, 1.0, e) / (1.0 + e)


def kernel(
    n_dp,
    n_tp,
    halves,
    stream_ref,
    history_ref,
    in_gain,
    adapter_hbm,
    key_hbm,
    query_hbm,
    value_hbm,
    gate_hbm,
    decay_up,
    rate_up,
    offset,
    head_gain,
    out_hbm,
    state_hbm,
    stream_out,
    state,
    wa,
    wk,
    wq,
    wv,
    wg,
    wo,
    sent,
    got,
    sq_sent,
    sq_got,
    mixed_all,
    terms,
    terms_got,
    fresh,
    x_ref,
    rows,
    splits,
    gather1,
    gather2,
    spread,
    load_sem,
    rs_send,
    rs_recv,
    sq_send,
    sq_recv,
    ag_send,
    ag_recv,
    tr_send,
    tr_recv,
    ta_send,
    ta_recv,
):
    me = lax.axis_index("dp")
    lane_me = lax.axis_index("tp")
    batch, depth = stream_ref.shape
    seq = batch // n_dp
    width = wk.shape[2]
    heads = width // HEAD
    span = batch // halves
    own = seq // halves
    count = own * heads
    part = span // n_tp
    rank = wa.shape[2] // 2
    vk = state.shape[2]
    tiles = vk // TILE
    lanes = sq_sent.shape[3]

    loads = {}

    def load(l, i, src, dst):
        loads[l, i] = pltpu.make_async_copy(src.at[l], dst.at[l], load_sem.at[l, i])
        loads[l, i].start()

    def load_in(l):
        load(l, 0, adapter_hbm, wa)
        load(l, 1, key_hbm, wk)
        load(l, 2, query_hbm, wq)
        load(l, 3, value_hbm, wv)
        load(l, 4, gate_hbm, wg)

    def load_rest(l):
        load(l, 5, state_hbm, state)
        load(l, 6, out_hbm, wo)

    load_in(0)
    load_rest(0)

    def dp_peer(o):
        return lax.rem(me + o, n_dp)

    def tp_peer(o):
        return lax.rem(lane_me + o, n_tp)

    barrier = pltpu.get_barrier_semaphore()
    for o in range(1, n_dp):
        pl.semaphore_signal(barrier, inc=1, device_id={"dp": dp_peer(o)}, device_id_type=MESH)
    for o in range(1, n_tp):
        pl.semaphore_signal(barrier, inc=1, device_id={"tp": tp_peer(o)}, device_id_type=MESH)

    def fill(t, carry):
        at = pl.ds(pl.multiple_of(t * TILE, TILE), TILE)
        r = (lax.broadcasted_iota(jnp.int32, (TILE, LANES), 0) + t * TILE) // HEAD
        c = lax.broadcasted_iota(jnp.int32, (TILE, LANES), 1)
        gather1[at, :] = jnp.where(r == c, 1.0, 0.0).astype(BF16)
        gather2[at, :] = jnp.where(r + HEAD == c, 1.0, 0.0).astype(BF16)
        r = lax.broadcasted_iota(jnp.int32, (LANES, TILE), 0)
        c = (lax.broadcasted_iota(jnp.int32, (LANES, TILE), 1) + t * TILE) // HEAD
        spread[:, at] = jnp.where((r == c) | (r == c + HEAD), 1.0, 0.0).astype(BF16)
        return carry

    low = lax.broadcasted_iota(jnp.int32, (own, LANES), 1) < HEAD
    low_rows = lax.broadcasted_iota(jnp.int32, (count, LANES), 1) < HEAD

    def to_rows(value, h, i):
        buf = rows.at[h, i]
        for j in range(width // LANES):
            pair = value[:, j * LANES : (j + 1) * LANES]
            turned = pltpu.roll(pair, HEAD, 1)
            buf[pl.ds(2 * j, own, stride=heads), :] = jnp.where(low, pair, turned)
            buf[pl.ds(2 * j + 1, own, stride=heads), :] = jnp.where(low, turned, pair)
        return rows[h, i]

    def half_sum(v):
        return jnp.sum(v, axis=1, keepdims=True) * 0.5

    def twice(v):
        return jnp.concatenate([v, v], axis=1)

    for h in range(halves):
        for d in range(n_dp):
            x_ref[h, d * own : (d + 1) * own, :] = stream_ref[d * seq + h * own : d * seq + (h + 1) * own, :].astype(F32)
    spans = jnp.floor(history_ref[...].astype(F32) * (1.0 / SPAN))
    phase = 0.5 + (spans - 3.0 * jnp.floor((spans + 0.5) * (1.0 / 3.0)))
    diagonal = lax.broadcasted_iota(jnp.int32, (seq, seq), 0) == lax.broadcasted_iota(jnp.int32, (seq, seq), 1)
    pos = jnp.sum(jnp.where(diagonal, phase, 0.0), axis=1, keepdims=True)
    mine = pl.ds(pl.multiple_of(me * own, own), own)
    own_part = pl.ds(pl.multiple_of(lane_me * part, part), part)
    row_at = lax.broadcasted_iota(jnp.int32, (span, lanes), 0)
    diag = row_at == lax.broadcasted_iota(jnp.int32, (span, lanes), 1)
    own_at = lax.broadcasted_iota(jnp.int32, (own, lanes), 0) + me * own
    own_diag = own_at == lax.broadcasted_iota(jnp.int32, (own, lanes), 1)
    sizes = [2 * rank, width, width, width, width]
    starts = [sum(sizes[:c]) for c in range(5)]
    pending = []

    def remote(src, dst, send, recv, where):
        copy = pltpu.make_async_remote_copy(
            src_ref=src, dst_ref=dst, send_sem=send, recv_sem=recv, device_id=where, device_id_type=MESH
        )
        copy.start()
        pending.append(copy)
        return copy

    copies = {}

    def project(l, h):
        x = x_ref[h]
        column = jnp.sum(x * x, axis=1, keepdims=True)
        line = jnp.sum(jnp.where(diag, column, 0.0), axis=0, keepdims=True)
        sq_sent[l, h] = jnp.broadcast_to(line, (8, lanes))
        scaled = (x * in_gain[l : l + 1, :]).astype(BF16)
        if l == 0 and h == 0:
            pl.semaphore_wait(barrier, n_dp + n_tp - 2)
        for o in range(1, n_dp):
            copies["sq", l, h, o] = remote(
                sq_sent.at[l, h],
                sq_got.at[l, h, o - 1],
                sq_send.at[l, h, o - 1],
                sq_recv.at[l, h, o - 1],
                {"dp": dp_peer(o)},
            )
        for c, weight in enumerate((wa, wk, wq, wv, wg)):
            if h == 0:
                loads[l, c].wait()
            cols = pl.ds(starts[c], sizes[c])
            sent[l, h, :, cols] = jnp.dot(scaled, weight[l], preferred_element_type=F32).astype(BF16)
            for o in range(1, n_dp):
                there = dp_peer(o)
                at = pl.ds(pl.multiple_of(there * own, own), own)
                copies["rs", l, h, c, o] = remote(
                    sent.at[l, h, at, cols],
                    got.at[l, h, o - 1, :, cols],
                    rs_send.at[l, h, c, o - 1],
                    rs_recv.at[l, h, c, o - 1],
                    {"dp": there},
                )

    def mix(l, h):
        for o in range(1, n_dp):
            copies["sq", l, h, o].wait_recv()
        line = sq_sent[l, h]
        for o in range(1, n_dp):
            line = line + sq_got[l, h, o - 1]
        squares = jnp.sum(jnp.where(own_diag, line[:1, :], 0.0), axis=1, keepdims=True)
        inv_rms = lax.rsqrt(squares / (depth * n_dp) + NORM_EPS)

        def total(c):
            for o in range(1, n_dp):
                copies["rs", l, h, c, o].wait_recv()
            cols = pl.ds(starts[c], sizes[c])
            out = sent[l, h, mine, cols].astype(F32)
            for o in range(1, n_dp):
                out = out + got[l, h, o - 1, :, cols].astype(F32)
            return out * inv_rms

        low_rank = total(0)
        z = offset[l : l + 1, :] + jnp.dot(
            jnp.tanh(low_rank[:, :rank]), decay_up[l], precision=lax.Precision.HIGHEST, preferred_element_type=F32
        )
        decay = to_rows(jnp.exp(sigmoid(z) * (-DECAY_SCALE) * pos[h * own : (h + 1) * own, :]), h, 0)
        learn = to_rows(
            sigmoid(
                jnp.dot(low_rank[:, rank:], rate_up[l], precision=lax.Precision.HIGHEST, preferred_element_type=F32)
            ),
            h,
            1,
        )
        keys = to_rows(total(1), h, 2)
        key_unit = keys * lax.rsqrt(half_sum(keys * keys) + 1.0)
        key_rate = key_unit * learn
        rows[h, 1] = key_rate
        query = to_rows(total(2), h, 3)
        key_query = half_sum(keys * query)
        rate_query = half_sum(key_rate * query)
        unit2 = twice(key_unit)
        query2 = twice(decay * query)
        if h == 0:
            loads[l, 5].wait()

        def products(t, acc):
            at = pl.ds(pl.multiple_of(t * TILE, TILE), TILE)
            s = state[l, h * count : (h + 1) * count, at]
            return (
                acc
                + jnp.dot((s * unit2).astype(BF16), gather1[at, :], preferred_element_type=F32)
                + jnp.dot((s * query2).astype(BF16), gather2[at, :], preferred_element_type=F32)
            )

        acc = lax.fori_loop(0, tiles, products, jnp.zeros((count, LANES), F32), unroll=True)
        turned = pltpu.roll(acc, HEAD, 1)
        state_key = jnp.where(low_rows, acc, turned)
        from_state = jnp.where(low_rows, turned, acc)
        value = to_rows(total(3), h, 4)
        readout = from_state - state_key * rate_query + value * key_query
        mean = half_sum(readout) * (1.0 / HEAD)
        centred = readout - mean
        var = half_sum(centred * centred) * (1.0 / HEAD)
        rows[h, 5] = centred * lax.rsqrt(var + GROUP_EPS)
        gate = sigmoid(total(4)) * head_gain[l : l + 1, :]
        normed = rows.at[h, 5]
        for j in range(width // LANES):
            even = normed[pl.ds(2 * j, own, stride=heads), :]
            odd = normed[pl.ds(2 * j + 1, own, stride=heads), :]
            cols = slice(j * LANES, (j + 1) * LANES)
            mixed_all[l, h, mine, cols] = (jnp.where(low, even, odd) * gate[:, cols]).astype(BF16)
        for o in range(1, n_dp):
            copies["ag", l, h, o] = remote(
                mixed_all.at[l, h, mine],
                mixed_all.at[l, h, mine],
                ag_send.at[l, h, o - 1],
                ag_recv.at[l, h, o - 1],
                {"dp": dp_peer(o)},
            )

        def split(v):
            high = v.astype(BF16)
            rest = (v - high.astype(F32)).astype(BF16)
            return jnp.where(low_rows, high.astype(F32), rest.astype(F32)).astype(BF16)

        splits[h, 0] = split(value)
        splits[h, 1] = split(state_key)

    def update(l, h, first, last):
        def one(t, carry):
            at = pl.ds(pl.multiple_of(t * TILE, TILE), TILE)
            wide = jnp.dot(splits[h, 0], spread[:, at], preferred_element_type=F32)
            drop = jnp.dot(splits[h, 1], spread[:, at], preferred_element_type=F32)
            block = slice(h * count, (h + 1) * count)
            state[l, block, at] = (
                state[l, block, at] * twice(rows[h, 0]) - drop * twice(rows[h, 1]) + wide * twice(rows[h, 2])
            )
            return carry

        lax.fori_loop(first, last, one, 0, unroll=True)

    def output(l, h):
        for o in range(1, n_dp):
            copies["ag", l, h, o].wait_recv()
        if h == 0:
            loads[l, 6].wait()
        product = jnp.dot(mixed_all[l, h], wo[l], preferred_element_type=F32)
        terms[l, h] = product.reshape(n_tp, part, depth).astype(BF16)
        for o in range(1, n_tp):
            there = tp_peer(o)
            copies["tr", l, h, o] = remote(
                terms.at[l, h, there],
                terms_got.at[l, h, o - 1],
                tr_send.at[l, h, o - 1],
                tr_recv.at[l, h, o - 1],
                {"tp": there},
            )

    def gather_terms(l, h):
        acc = terms[l, h, lane_me].astype(F32)
        for o in range(1, n_tp):
            copies["tr", l, h, o].wait_recv()
            acc = acc + terms_got[l, h, o - 1].astype(F32)
        fresh[l, h, lane_me] = (x_ref[h, own_part, :] + acc).astype(BF16)
        for o in range(1, n_tp):
            copies["ta", l, h, o] = remote(
                fresh.at[l, h, lane_me],
                fresh.at[l, h, lane_me],
                ta_send.at[l, h, o - 1],
                ta_recv.at[l, h, o - 1],
                {"tp": tp_peer(o)},
            )

    def renew(l, h):
        for o in range(1, n_tp):
            copies["ta", l, h, o].wait_recv()
        if l + 1 < BLOCK_COUNT:
            x_ref[h] = fresh[l, h].astype(F32).reshape(span, depth)
        else:
            last = fresh[l, h].reshape(span, depth)
            for d in range(n_dp):
                stream_out[d * seq + h * own : d * seq + (h + 1) * own, :] = last[d * own : (d + 1) * own, :]

    every = range(halves)
    cut = [tiles * i // 4 for i in range(5)]
    for l in range(BLOCK_COUNT):
        for h in every:
            if l > 0:
                renew(l - 1, h)
            project(l, h)
        if l == 0:
            lax.fori_loop(0, tiles, fill, 0)
        if l + 1 < BLOCK_COUNT:
            load_in(l + 1)
            load_rest(l + 1)
        for h in every:
            mix(l, h)
        for h in every:
            update(l, h, cut[0], cut[1])
            output(l, h)
        for h in every:
            update(l, h, cut[1], cut[2])
        for h in every:
            update(l, h, cut[2], cut[3])
            gather_terms(l, h)
        for h in every:
            update(l, h, cut[3], cut[4])
    for h in every:
        renew(BLOCK_COUNT - 1, h)
    for copy in pending:
        copy.wait_send()


def flush(out, state, out_hbm, state_hbm, sem):
    copies = [pltpu.make_async_copy(out, out_hbm, sem.at[0])]
    for i in range(FLUSHES):
        rows = state.shape[1] // FLUSHES
        at = pl.ds(i * rows, rows)
        copies.append(pltpu.make_async_copy(state.at[:, at], state_hbm.at[:, at], sem.at[i + 1]))
    for copy in copies:
        copy.start()
    for copy in copies:
        copy.wait()


def solution(mesh):
    n_dp, n_tp = mesh.shape["dp"], mesh.shape["tp"]

    def body(
        stream,
        history,
        input_norm_gain,
        query_weight,
        key_weight,
        value_weight,
        gate_weight,
        adapter_down_weight,
        decay_up_weight,
        rate_up_weight,
        decay_offset,
        head_norm_gain,
        output_weight,
        recurrent_state,
    ):
        batch, depth = stream.shape
        width = query_weight.shape[2]
        blocks, seq, heads, vk = recurrent_state.shape
        count = seq * heads
        halves = 2 if batch % (2 * 8 * n_tp) == 0 and seq % 32 == 0 else 1
        span = batch // halves
        own = seq // halves
        part = span // n_tp
        lanes = (span + LANES - 1) // LANES * LANES
        columns = 4 * width + adapter_down_weight.shape[2]
        vmem = pl.BlockSpec(memory_space=pltpu.VMEM)
        hbm = pl.BlockSpec(memory_space=pl.ANY)
        dma = pltpu.SemaphoreType.DMA

        def like(w):
            return pltpu.VMEM(w.shape, w.dtype)

        out, new_state = pl.pallas_call(
            functools.partial(kernel, n_dp, n_tp, halves),
            out_shape=(
                pltpu.VMEM((batch, depth), BF16),
                pltpu.VMEM((blocks, count, vk), F32),
            ),
            in_specs=[vmem] * 3 + [hbm] * 5 + [vmem] * 4 + [hbm] * 2,
            out_specs=(vmem, vmem),
            scratch_shapes=[
                like(adapter_down_weight),
                like(key_weight),
                like(query_weight),
                like(value_weight),
                like(gate_weight),
                like(output_weight),
                pltpu.VMEM((blocks, halves, span, columns), BF16),
                pltpu.VMEM((blocks, halves, n_dp - 1, own, columns), BF16),
                pltpu.VMEM((blocks, halves, 8, lanes), F32),
                pltpu.VMEM((blocks, halves, n_dp - 1, 8, lanes), F32),
                pltpu.VMEM((blocks, halves, span, width), BF16),
                pltpu.VMEM((blocks, halves, n_tp, part, depth), BF16),
                pltpu.VMEM((blocks, halves, n_tp - 1, part, depth), BF16),
                pltpu.VMEM((blocks, halves, n_tp, part, depth), BF16),
                pltpu.VMEM((halves, span, depth), F32),
                pltpu.VMEM((halves, 6, count // halves, LANES), F32),
                pltpu.VMEM((halves, 2, count // halves, LANES), BF16),
                pltpu.VMEM((vk, LANES), BF16),
                pltpu.VMEM((vk, LANES), BF16),
                pltpu.VMEM((LANES, vk), BF16),
                dma((blocks, 7)),
                dma((blocks, halves, 5, n_dp - 1)),
                dma((blocks, halves, 5, n_dp - 1)),
                dma((blocks, halves, n_dp - 1)),
                dma((blocks, halves, n_dp - 1)),
                dma((blocks, halves, n_dp - 1)),
                dma((blocks, halves, n_dp - 1)),
                dma((blocks, halves, n_tp - 1)),
                dma((blocks, halves, n_tp - 1)),
                dma((blocks, halves, n_tp - 1)),
                dma((blocks, halves, n_tp - 1)),
            ],
            compiler_params=pltpu.CompilerParams(
                collective_id=0, has_side_effects=True, vmem_limit_bytes=54 * 1024 * 1024
            ),
        )(
            stream,
            history[None, :],
            input_norm_gain,
            adapter_down_weight,
            key_weight,
            query_weight,
            value_weight,
            gate_weight,
            decay_up_weight,
            rate_up_weight,
            decay_offset,
            head_norm_gain,
            output_weight,
            recurrent_state.reshape(blocks, count, vk),
        )
        out, new_state = pl.pallas_call(
            flush,
            out_shape=(
                jax.ShapeDtypeStruct((batch, depth), BF16),
                jax.ShapeDtypeStruct((blocks, count, vk), F32),
            ),
            in_specs=[hbm, hbm],
            out_specs=(hbm, hbm),
            scratch_shapes=[dma((FLUSHES + 1,))],
            compiler_params=pltpu.CompilerParams(vmem_limit_bytes=1024 * 1024),
        )(out, new_state)
        return out, new_state.reshape(blocks, seq, heads, vk)

    placed = (
        P(None, "dp"),
        P("dp"),
        P(None, "dp"),
        P(None, "dp", "tp"),
        P(None, "dp", "tp"),
        P(None, "dp", "tp"),
        P(None, "dp", "tp"),
        P(None, "dp", None),
        P(None, None, "tp"),
        P(None, None, "tp"),
        P(None, "tp"),
        P(None, "tp"),
        P(None, "tp", "dp"),
        P(None, "dp", "tp", None),
    )
    return jax.shard_map(
        body,
        mesh=mesh,
        in_specs=placed,
        out_specs=(P(None, "dp"), P(None, "dp", "tp", None)),
        check_vma=False,
    )
```

time: 63.8 us -> 58.6 us (0.918)
  local copies, waits for them, and re-layouts: 4.11 us -> 0 us
  Pallas kernels: 58.9 us -> 57.9 us
    unnamed x4 -> x0, local copies, waits for them, and re-layouts: 4.11 us -> none
    pallas_call x1 -> x2, Pallas kernels: 58.9 us -> 57.9 us  [the longest x1 54.4 us: body(): pl.pallas_call(functools.partial(kernel, n_dp, n_tp, halves), out_shape=(...]
where the time goes in v1:
time: 58.6 us; the launch traced here: 58.5 us
  Pallas kernels  57.9 us (99%)
  between operations  0.64 us (1%)
    pallas_call x1, Pallas kernels, body(): pl.pallas_call(functools.partial(kernel, n_dp, n_tp, halves), out_shape=(...  54.4 us
    pallas_call x1, Pallas kernels, body(): pl.pallas_call(flush, out_shape=(jax.ShapeDtypeStruct((batch, depth), BF1...  3.46 us

profile of v1, /device:TPU:0, one launch (start us, length us, event | category | flops | bytes accessed | tf_op | source)
XLA Modules:
  0.0 58.5 jit_solution(13641656095967722856)
XLA Ops:
  0.6 54.4 %shard_map.149 = (bf16[128,1024]{1,0:T(8,128)(2,1)S(1)}, f32[2,256,4096]{2,1,0:T(8,128)S(1)}) custom-call(bf16[128,1024]{1,0:T(8,128)(2,1)} %stream_ref.1, s32[1,32]{1,0:T(1,128)} %bitcast.4, f32[2,1024]{1,0:T(2,128)} %in_gain.1, bf16[2,1024,128]{2,1,0:T(8,128)(2,1)} %adapter_hbm.1, bf16[2,1024,512]{2,1,0:T(8,128)(2,1)} %key_hbm.1, ...), custom_call_target="tpu_custom_call" | custom-call | tf_op jit(solution)/shard_map/pallas_call | solution.py:434
  55.0 3.5 %shard_map.150 = (bf16[128,1024]{1,0:T(8,128)(2,1)}, f32[2,256,4096]{2,1,0:T(8,128)}) custom-call(bf16[128,1024]{1,0:T(8,128)(2,1)S(1)} %get-tuple-element.6.out, f32[2,256,4096]{2,1,0:T(8,128)S(1)} %get-tuple-element.7.state), custom_call_target="tpu_custom_call" | custom-call | tf_op jit(solution)/shard_map/pallas_call | solution.py:494

commit v2 on v1

--- a/solution.py
+++ b/solution.py
@@ -16,6 +16,7 @@
 DECAY_SCALE = 0.6065306597126334
 TILE = 256
 FLUSHES = 8
+PIECES = 2
 MESH = pl.DeviceIdType.MESH
 F32 = jnp.float32
 BF16 = jnp.bfloat16
@@ -30,22 +31,29 @@
     n_dp,
     n_tp,
     halves,
-    stream_ref,
-    history_ref,
-    in_gain,
+    stream_hbm,
+    history_hbm,
+    in_gain_hbm,
     adapter_hbm,
     key_hbm,
     query_hbm,
     value_hbm,
     gate_hbm,
+    decay_up_hbm,
+    rate_up_hbm,
+    offset_hbm,
+    head_gain_hbm,
+    out_hbm,
+    state_hbm,
+    stream_out,
+    state,
+    stream_ref,
+    history_ref,
+    in_gain,
     decay_up,
     rate_up,
     offset,
     head_gain,
-    out_hbm,
-    state_hbm,
-    stream_out,
-    state,
     wa,
     wk,
     wq,
@@ -66,6 +74,7 @@
     gather1,
     gather2,
     spread,
+    small_sem,
     load_sem,
     rs_send,
     rs_recv,
@@ -87,17 +96,36 @@
     span = batch // halves
     own = seq // halves
     count = own * heads
-    part = span // n_tp
     rank = wa.shape[2] // 2
     vk = state.shape[2]
     tiles = vk // TILE
     lanes = sq_sent.shape[3]
+    reducers, part_rows, part_cols = terms.shape[2:]
+    first = (n_tp - reducers) // 2
+    strips = depth // part_cols
+
+    def dp_peer(o):
+        return lax.rem(me + o, n_dp)
+
+    def tp_peer(o):
+        return lax.rem(lane_me + o, n_tp)
+
+    barrier = pltpu.get_barrier_semaphore()
+    for o in range(1, n_tp):
+        pl.semaphore_signal(barrier, inc=1, device_id={"tp": tp_peer(o)}, device_id_type=MESH)
+    for o in range(1, n_dp):
+        pl.semaphore_signal(barrier, inc=1, device_id={"dp": dp_peer(o)}, device_id_type=MESH)
 
     loads = {}
+    small = []
 
     def load(l, i, src, dst):
         loads[l, i] = pltpu.make_async_copy(src.at[l], dst.at[l], load_sem.at[l, i])
         loads[l, i].start()
+
+    def load_small(src, dst):
+        small.append(pltpu.make_async_copy(src, dst, small_sem.at[len(small)]))
+        small[-1].start()
 
     def load_in(l):
         load(l, 0, adapter_hbm, wa)
@@ -110,20 +138,15 @@
         load(l, 5, state_hbm, state)
         load(l, 6, out_hbm, wo)
 
+    load_small(stream_hbm, stream_ref)
+    load_small(in_gain_hbm, in_gain)
     load_in(0)
+    load_small(history_hbm, history_ref)
+    load_small(decay_up_hbm, decay_up)
+    load_small(rate_up_hbm, rate_up)
+    load_small(offset_hbm, offset)
+    load_small(head_gain_hbm, head_gain)
     load_rest(0)
-
-    def dp_peer(o):
-        return lax.rem(me + o, n_dp)
-
-    def tp_peer(o):
-        return lax.rem(lane_me + o, n_tp)
-
-    barrier = pltpu.get_barrier_semaphore()
-    for o in range(1, n_dp):
-        pl.semaphore_signal(barrier, inc=1, device_id={"dp": dp_peer(o)}, device_id_type=MESH)
-    for o in range(1, n_tp):
-        pl.semaphore_signal(barrier, inc=1, device_id={"tp": tp_peer(o)}, device_id_type=MESH)
 
     def fill(t, carry):
         at = pl.ds(pl.multiple_of(t * TILE, TILE), TILE)
@@ -154,64 +177,99 @@
     def twice(v):
         return jnp.concatenate([v, v], axis=1)
 
-    for h in range(halves):
-        for d in range(n_dp):
-            x_ref[h, d * own : (d + 1) * own, :] = stream_ref[d * seq + h * own : d * seq + (h + 1) * own, :].astype(F32)
-    spans = jnp.floor(history_ref[...].astype(F32) * (1.0 / SPAN))
-    phase = 0.5 + (spans - 3.0 * jnp.floor((spans + 0.5) * (1.0 / 3.0)))
-    diagonal = lax.broadcasted_iota(jnp.int32, (seq, seq), 0) == lax.broadcasted_iota(jnp.int32, (seq, seq), 1)
-    pos = jnp.sum(jnp.where(diagonal, phase, 0.0), axis=1, keepdims=True)
     mine = pl.ds(pl.multiple_of(me * own, own), own)
-    own_part = pl.ds(pl.multiple_of(lane_me * part, part), part)
     row_at = lax.broadcasted_iota(jnp.int32, (span, lanes), 0)
     diag = row_at == lax.broadcasted_iota(jnp.int32, (span, lanes), 1)
     own_at = lax.broadcasted_iota(jnp.int32, (own, lanes), 0) + me * own
     own_diag = own_at == lax.broadcasted_iota(jnp.int32, (own, lanes), 1)
     sizes = [2 * rank, width, width, width, width]
     starts = [sum(sizes[:c]) for c in range(5)]
-    pending = []
-
-    def remote(src, dst, send, recv, where):
-        copy = pltpu.make_async_remote_copy(
+    copies = {}
+
+    def describe(key, src, dst, send, recv, where):
+        copies[key] = pltpu.make_async_remote_copy(
             src_ref=src, dst_ref=dst, send_sem=send, recv_sem=recv, device_id=where, device_id_type=MESH
         )
-        copy.start()
-        pending.append(copy)
-        return copy
-
-    copies = {}
-
-    def project(l, h):
-        x = x_ref[h]
-        column = jnp.sum(x * x, axis=1, keepdims=True)
-        line = jnp.sum(jnp.where(diag, column, 0.0), axis=0, keepdims=True)
-        sq_sent[l, h] = jnp.broadcast_to(line, (8, lanes))
-        scaled = (x * in_gain[l : l + 1, :]).astype(BF16)
-        if l == 0 and h == 0:
-            pl.semaphore_wait(barrier, n_dp + n_tp - 2)
+        return copies[key]
+
+    def send_squares(l, h):
         for o in range(1, n_dp):
-            copies["sq", l, h, o] = remote(
+            describe(
+                ("sq", l, h, o),
                 sq_sent.at[l, h],
                 sq_got.at[l, h, o - 1],
                 sq_send.at[l, h, o - 1],
                 sq_recv.at[l, h, o - 1],
                 {"dp": dp_peer(o)},
-            )
-        for c, weight in enumerate((wa, wk, wq, wv, wg)):
+            ).start()
+
+    def send_columns(l, h, c):
+        cols = pl.ds(starts[c], sizes[c])
+        for o in range(1, n_dp):
+            there = dp_peer(o)
+            at = pl.ds(pl.multiple_of(there * own, own), own)
+            describe(
+                ("rs", l, h, c, o),
+                sent.at[l, h, at, cols],
+                got.at[l, h, o - 1, :, cols],
+                rs_send.at[l, h, c, o - 1],
+                rs_recv.at[l, h, c, o - 1],
+                {"dp": there},
+            ).start()
+
+    def put_squares(l, h, x):
+        column = jnp.sum(x * x, axis=1, keepdims=True)
+        line = jnp.sum(jnp.where(diag, column, 0.0), axis=0, keepdims=True)
+        sq_sent[l, h] = jnp.broadcast_to(line, (8, lanes))
+
+    weights = (wa, wk, wq, wv, wg)
+
+    def project_all():
+        small[0].wait()
+        small[1].wait()
+        for h in range(halves):
+            for d in range(n_dp):
+                x_ref[h, d * own : (d + 1) * own, :] = stream_ref[
+                    d * seq + h * own : d * seq + (h + 1) * own, :
+                ]
+        for h in range(halves):
+            put_squares(0, h, x_ref[h].astype(F32))
+        x = x_ref[...].reshape(batch, depth).astype(F32)
+        scaled = (x * in_gain[:1, :]).astype(BF16)
+        for c, weight in enumerate(weights):
+            loads[0, c].wait()
+            cols = pl.ds(starts[c], sizes[c])
+            product = jnp.dot(scaled, weight[0], preferred_element_type=F32).astype(BF16)
+            sent[0, :, :, cols] = product.reshape(halves, span, sizes[c])
+        pl.semaphore_wait(barrier, n_dp + n_tp - 2)
+        for h in range(halves):
+            send_squares(0, h)
+            for c in range(len(weights)):
+                send_columns(0, h, c)
+
+    def project(l, h):
+        rows_of = []
+        for i in range(reducers // strips):
+            strip = [fresh[l - 1, h, i * strips + j] for j in range(strips)]
+            rows_of.append(jnp.concatenate(strip, axis=1))
+        x = jnp.concatenate(rows_of, axis=0).astype(F32)
+        put_squares(l, h, x)
+        scaled = (x * in_gain[l : l + 1, :]).astype(BF16)
+        send_squares(l, h)
+        for c, weight in enumerate(weights):
             if h == 0:
                 loads[l, c].wait()
             cols = pl.ds(starts[c], sizes[c])
             sent[l, h, :, cols] = jnp.dot(scaled, weight[l], preferred_element_type=F32).astype(BF16)
-            for o in range(1, n_dp):
-                there = dp_peer(o)
-                at = pl.ds(pl.multiple_of(there * own, own), own)
-                copies["rs", l, h, c, o] = remote(
-                    sent.at[l, h, at, cols],
-                    got.at[l, h, o - 1, :, cols],
-                    rs_send.at[l, h, c, o - 1],
-                    rs_recv.at[l, h, c, o - 1],
-                    {"dp": there},
-                )
+            send_columns(l, h, c)
+
+    def prepare():
+        for copy in small[2:]:
+            copy.wait()
+        spans = jnp.floor(history_ref[...].astype(F32) * (1.0 / SPAN))
+        phase = 0.5 + (spans - 3.0 * jnp.floor((spans + 0.5) * (1.0 / 3.0)))
+        diagonal = lax.broadcasted_iota(jnp.int32, (seq, seq), 0) == lax.broadcasted_iota(jnp.int32, (seq, seq), 1)
+        return jnp.sum(jnp.where(diagonal, phase, 0.0), axis=1, keepdims=True)
 
     def mix(l, h):
         for o in range(1, n_dp):
@@ -282,13 +340,14 @@
             cols = slice(j * LANES, (j + 1) * LANES)
             mixed_all[l, h, mine, cols] = (jnp.where(low, even, odd) * gate[:, cols]).astype(BF16)
         for o in range(1, n_dp):
-            copies["ag", l, h, o] = remote(
+            describe(
+                ("ag", l, h, o),
                 mixed_all.at[l, h, mine],
                 mixed_all.at[l, h, mine],
                 ag_send.at[l, h, o - 1],
                 ag_recv.at[l, h, o - 1],
                 {"dp": dp_peer(o)},
-            )
+            ).start()
 
         def split(v):
             high = v.astype(BF16)
@@ -316,71 +375,120 @@
             copies["ag", l, h, o].wait_recv()
         if h == 0:
             loads[l, 6].wait()
-        product = jnp.dot(mixed_all[l, h], wo[l], preferred_element_type=F32)
-        terms[l, h] = product.reshape(n_tp, part, depth).astype(BF16)
+        product = jnp.dot(mixed_all[l, h], wo[l], preferred_element_type=F32).astype(BF16)
+        for k in range(reducers):
+            i, j = k // strips, k % strips
+            terms[l, h, k] = product[
+                i * part_rows : (i + 1) * part_rows, j * part_cols : (j + 1) * part_cols
+            ]
+        for k in range(reducers):
+            copy = describe(
+                ("tr", l, h, k),
+                terms.at[l, h, k],
+                terms_got.at[l, h, lane_me],
+                tr_send.at[l, h, k],
+                tr_recv.at[l, h, lane_me],
+                {"tp": first + k},
+            )
+            pl.when(lane_me != first + k)(copy.start)
+
+    reducing = (lane_me >= first) & (lane_me < first + reducers)
+    slot = jnp.clip(lane_me - first, 0, reducers - 1)
+
+    def gather_terms(l, h):
         for o in range(1, n_tp):
-            there = tp_peer(o)
-            copies["tr", l, h, o] = remote(
-                terms.at[l, h, there],
-                terms_got.at[l, h, o - 1],
-                tr_send.at[l, h, o - 1],
-                tr_recv.at[l, h, o - 1],
-                {"tp": there},
-            )
-
-    def gather_terms(l, h):
-        acc = terms[l, h, lane_me].astype(F32)
-        for o in range(1, n_tp):
-            copies["tr", l, h, o].wait_recv()
-            acc = acc + terms_got[l, h, o - 1].astype(F32)
-        fresh[l, h, lane_me] = (x_ref[h, own_part, :] + acc).astype(BF16)
-        for o in range(1, n_tp):
-            copies["ta", l, h, o] = remote(
-                fresh.at[l, h, lane_me],
-                fresh.at[l, h, lane_me],
+            describe(
+                ("ta", l, h, o),
+                fresh.at[l, h, slot],
+                fresh.at[l, h, slot],
                 ta_send.at[l, h, o - 1],
-                ta_recv.at[l, h, o - 1],
+                ta_recv.at[l, h, slot],
                 {"tp": tp_peer(o)},
             )
 
+        @pl.when(reducing)
+        def _():
+            acc = terms[l, h, slot].astype(F32)
+            if l == 0:
+                at_rows = pl.ds(pl.multiple_of(slot // strips * part_rows, part_rows), part_rows)
+                at_cols = pl.ds(pl.multiple_of(slot % strips * part_cols, part_cols), part_cols)
+                acc = acc + x_ref[h, at_rows, at_cols].astype(F32)
+            else:
+                acc = acc + fresh[l - 1, h, slot].astype(F32)
+            for o in range(1, n_tp):
+                there = tp_peer(o)
+                pltpu.make_async_remote_copy(
+                    src_ref=terms.at[l, h, slot],
+                    dst_ref=terms_got.at[l, h, there],
+                    send_sem=tr_send.at[l, h, slot],
+                    recv_sem=tr_recv.at[l, h, there],
+                    device_id={"tp": there},
+                    device_id_type=MESH,
+                ).wait_recv()
+                acc = acc + terms_got[l, h, there].astype(F32)
+            fresh[l, h, slot] = acc.astype(BF16)
+            for o in range(1, n_tp):
+                copies["ta", l, h, o].start()
+
     def renew(l, h):
-        for o in range(1, n_tp):
-            copies["ta", l, h, o].wait_recv()
-        if l + 1 < BLOCK_COUNT:
-            x_ref[h] = fresh[l, h].astype(F32).reshape(span, depth)
-        else:
-            last = fresh[l, h].reshape(span, depth)
+        for k in range(reducers):
+            copy = pltpu.make_async_remote_copy(
+                src_ref=fresh.at[l, h, k],
+                dst_ref=fresh.at[l, h, k],
+                send_sem=ta_send.at[l, h, 0],
+                recv_sem=ta_recv.at[l, h, k],
+                device_id={"tp": tp_peer(1)},
+                device_id_type=MESH,
+            )
+            pl.when(lane_me != first + k)(copy.wait_recv)
+
+    def finish(h):
+        for i in range(reducers // strips):
+            strip = [fresh[BLOCK_COUNT - 1, h, i * strips + j] for j in range(strips)]
+            value = jnp.concatenate(strip, axis=1)
             for d in range(n_dp):
-                stream_out[d * seq + h * own : d * seq + (h + 1) * own, :] = last[d * own : (d + 1) * own, :]
+                low_row, high_row = max(d * own, i * part_rows), min((d + 1) * own, (i + 1) * part_rows)
+                if low_row < high_row:
+                    to = d * (seq - own) + h * own
+                    stream_out[to + low_row : to + high_row, :] = value[
+                        low_row - i * part_rows : high_row - i * part_rows, :
+                    ]
 
     every = range(halves)
-    cut = [tiles * i // 4 for i in range(5)]
+    cut = [tiles * i // 2 for i in range(3)]
+    project_all()
+    lax.fori_loop(0, tiles, fill, 0)
+    pos = prepare()
     for l in range(BLOCK_COUNT):
-        for h in every:
-            if l > 0:
+        if l > 0:
+            for h in every:
                 renew(l - 1, h)
-            project(l, h)
-        if l == 0:
-            lax.fori_loop(0, tiles, fill, 0)
+                project(l, h)
         if l + 1 < BLOCK_COUNT:
             load_in(l + 1)
             load_rest(l + 1)
         for h in every:
             mix(l, h)
         for h in every:
+            output(l, h)
             update(l, h, cut[0], cut[1])
-            output(l, h)
         for h in every:
+            gather_terms(l, h)
             update(l, h, cut[1], cut[2])
-        for h in every:
-            update(l, h, cut[2], cut[3])
-            gather_terms(l, h)
-        for h in every:
-            update(l, h, cut[3], cut[4])
     for h in every:
         renew(BLOCK_COUNT - 1, h)
-    for copy in pending:
-        copy.wait_send()
+        finish(h)
+    for key, copy in copies.items():
+        if key[0] == "tr":
+            pl.when(lane_me != first + key[3])(copy.wait_send)
+        elif key[0] != "ta":
+            copy.wait_send()
+
+    @pl.when(reducing)
+    def _():
+        for key, copy in copies.items():
+            if key[0] == "ta":
+                copy.wait_send()
 
 
 def flush(out, state, out_hbm, state_hbm, sem):
@@ -418,11 +526,13 @@
         width = query_weight.shape[2]
         blocks, seq, heads, vk = recurrent_state.shape
         count = seq * heads
-        halves = 2 if batch % (2 * 8 * n_tp) == 0 and seq % 32 == 0 else 1
+        halves = PIECES if seq % (8 * PIECES) == 0 else 1
         span = batch // halves
         own = seq // halves
-        part = span // n_tp
         lanes = (span + LANES - 1) // LANES * LANES
+        reducers = n_tp // 2 if n_tp % 4 == 0 else n_tp
+        strips = min(reducers, depth // LANES)
+        part_rows, part_cols = span * strips // reducers, depth // strips
         columns = 4 * width + adapter_down_weight.shape[2]
         vmem = pl.BlockSpec(memory_space=pltpu.VMEM)
         hbm = pl.BlockSpec(memory_space=pl.ANY)
@@ -437,9 +547,16 @@
                 pltpu.VMEM((batch, depth), BF16),
                 pltpu.VMEM((blocks, count, vk), F32),
             ),
-            in_specs=[vmem] * 3 + [hbm] * 5 + [vmem] * 4 + [hbm] * 2,
+            in_specs=[hbm] * 14,
             out_specs=(vmem, vmem),
             scratch_shapes=[
+                like(stream),
+                pltpu.VMEM((1, seq), history.dtype),
+                like(input_norm_gain),
+                like(decay_up_weight),
+                like(rate_up_weight),
+                like(decay_offset),
+                like(head_norm_gain),
                 like(adapter_down_weight),
                 like(key_weight),
                 like(query_weight),
@@ -451,15 +568,16 @@
                 pltpu.VMEM((blocks, halves, 8, lanes), F32),
                 pltpu.VMEM((blocks, halves, n_dp - 1, 8, lanes), F32),
                 pltpu.VMEM((blocks, halves, span, width), BF16),
-                pltpu.VMEM((blocks, halves, n_tp, part, depth), BF16),
-                pltpu.VMEM((blocks, halves, n_tp - 1, part, depth), BF16),
-                pltpu.VMEM((blocks, halves, n_tp, part, depth), BF16),
-                pltpu.VMEM((halves, span, depth), F32),
+                pltpu.VMEM((blocks, halves, reducers, part_rows, part_cols), BF16),
+                pltpu.VMEM((blocks, halves, n_tp, part_rows, part_cols), BF16),
+                pltpu.VMEM((blocks, halves, reducers, part_rows, part_cols), BF16),
+                pltpu.VMEM((halves, span, depth), BF16),
                 pltpu.VMEM((halves, 6, count // halves, LANES), F32),
                 pltpu.VMEM((halves, 2, count // halves, LANES), BF16),
                 pltpu.VMEM((vk, LANES), BF16),
                 pltpu.VMEM((vk, LANES), BF16),
                 pltpu.VMEM((LANES, vk), BF16),
+                dma((7,)),
                 dma((blocks, 7)),
                 dma((blocks, halves, 5, n_dp - 1)),
                 dma((blocks, halves, 5, n_dp - 1)),
@@ -467,10 +585,10 @@
                 dma((blocks, halves, n_dp - 1)),
                 dma((blocks, halves, n_dp - 1)),
                 dma((blocks, halves, n_dp - 1)),
+                dma((blocks, halves, reducers)),
+                dma((blocks, halves, n_tp)),
                 dma((blocks, halves, n_tp - 1)),
-                dma((blocks, halves, n_tp - 1)),
-                dma((blocks, halves, n_tp - 1)),
-                dma((blocks, halves, n_tp - 1)),
+                dma((blocks, halves, reducers)),
             ],
             compiler_params=pltpu.CompilerParams(
                 collective_id=0, has_side_effects=True, vmem_limit_bytes=54 * 1024 * 1024

time: 58.6 us -> 54.9 us (0.937)
  Pallas kernels: 57.9 us -> 54.2 us
    pallas_call x1, Pallas kernels: 54.4 us -> 50.7 us  [body(): pl.pallas_call(functools.partial(kernel, n_dp, n_tp, halves), out_shape=(...]
where the time goes in v2:
time: 54.9 us; the launch traced here: 54.8 us
  Pallas kernels  54.2 us (99%)
  between operations  0.64 us (1%)
    pallas_call x1, Pallas kernels, body(): pl.pallas_call(functools.partial(kernel, n_dp, n_tp, halves), out_shape=(...  50.7 us
    pallas_call x1, Pallas kernels, body(): pl.pallas_call(flush, out_shape=(jax.ShapeDtypeStruct((batch, depth), BF1...  3.46 us

profile of v2, /device:TPU:0, one launch (start us, length us, event | category | flops | bytes accessed | tf_op | source)
XLA Modules:
  0.0 54.8 jit_solution(17032276145275865873)
XLA Ops:
  0.6 50.7 %shard_map.149 = (bf16[128,1024]{1,0:T(8,128)(2,1)S(1)}, f32[2,256,4096]{2,1,0:T(8,128)S(1)}) custom-call(bf16[128,1024]{1,0:T(8,128)(2,1)} %stream_hbm.1, s32[1,32]{1,0:T(1,128)} %bitcast.4, f32[2,1024]{1,0:T(2,128)} %in_gain_hbm.1, bf16[2,1024,128]{2,1,0:T(8,128)(2,1)} %adapter_hbm.1, bf16[2,1024,512]{2,1,0:T(8,128)(2,1)} %key_hbm.1, ...), custom_call_target="tpu_custom_call" | custom-call | tf_op jit(solution)/shard_map/pallas_call | solution.py:544
  51.3 3.5 %shard_map.150 = (bf16[128,1024]{1,0:T(8,128)(2,1)}, f32[2,256,4096]{2,1,0:T(8,128)}) custom-call(bf16[128,1024]{1,0:T(8,128)(2,1)S(1)} %get-tuple-element.6.out, f32[2,256,4096]{2,1,0:T(8,128)S(1)} %get-tuple-element.7.state), custom_call_target="tpu_custom_call" | custom-call | tf_op jit(solution)/shard_map/pallas_call | solution.py:612

commit v3 on v2

--- a/solution.py
+++ b/solution.py
@@ -17,6 +17,7 @@
 TILE = 256
 FLUSHES = 8
 PIECES = 2
+GROUPS = ((0,), (1,), (2,), (3,), (4,))
 MESH = pl.DeviceIdType.MESH
 F32 = jnp.float32
 BF16 = jnp.bfloat16
@@ -184,37 +185,31 @@
     own_diag = own_at == lax.broadcasted_iota(jnp.int32, (own, lanes), 1)
     sizes = [2 * rank, width, width, width, width]
     starts = [sum(sizes[:c]) for c in range(5)]
-    copies = {}
-
-    def describe(key, src, dst, send, recv, where):
-        copies[key] = pltpu.make_async_remote_copy(
+    def copy_of(src, dst, send, recv, where):
+        return pltpu.make_async_remote_copy(
             src_ref=src, dst_ref=dst, send_sem=send, recv_sem=recv, device_id=where, device_id_type=MESH
         )
-        return copies[key]
+
+    def arrived(ref, recv):
+        copy_of(ref, ref, tr_send, recv, {"tp": tp_peer(1)}).wait_recv()
+
+    def left(ref, send):
+        copy_of(ref, ref, send, ta_recv.at[0, 0], {"tp": tp_peer(1)}).wait_send()
 
     def send_squares(l, h):
         for o in range(1, n_dp):
-            describe(
-                ("sq", l, h, o),
-                sq_sent.at[l, h],
-                sq_got.at[l, h, o - 1],
-                sq_send.at[l, h, o - 1],
-                sq_recv.at[l, h, o - 1],
-                {"dp": dp_peer(o)},
-            ).start()
-
-    def send_columns(l, h, c):
-        cols = pl.ds(starts[c], sizes[c])
+            copy_of(sq_sent.at[l, h], sq_got.at[l, h, o - 1], sq_send, sq_recv.at[l, h], {"dp": dp_peer(o)}).start()
+
+    def columns_of(g):
+        return pl.ds(starts[GROUPS[g][0]], sum(sizes[c] for c in GROUPS[g]))
+
+    def send_columns(l, h, g):
+        cols = columns_of(g)
         for o in range(1, n_dp):
             there = dp_peer(o)
             at = pl.ds(pl.multiple_of(there * own, own), own)
-            describe(
-                ("rs", l, h, c, o),
-                sent.at[l, h, at, cols],
-                got.at[l, h, o - 1, :, cols],
-                rs_send.at[l, h, c, o - 1],
-                rs_recv.at[l, h, c, o - 1],
-                {"dp": there},
+            copy_of(
+                sent.at[l, h, at, cols], got.at[l, h, o - 1, :, cols], rs_send, rs_recv.at[l, h, g], {"dp": there}
             ).start()
 
     def put_squares(l, h, x):
@@ -244,8 +239,8 @@
         pl.semaphore_wait(barrier, n_dp + n_tp - 2)
         for h in range(halves):
             send_squares(0, h)
-            for c in range(len(weights)):
-                send_columns(0, h, c)
+            for g in range(len(GROUPS)):
+                send_columns(0, h, g)
 
     def project(l, h):
         rows_of = []
@@ -261,7 +256,9 @@
                 loads[l, c].wait()
             cols = pl.ds(starts[c], sizes[c])
             sent[l, h, :, cols] = jnp.dot(scaled, weight[l], preferred_element_type=F32).astype(BF16)
-            send_columns(l, h, c)
+            for g in range(len(GROUPS)):
+                if GROUPS[g][-1] == c:
+                    send_columns(l, h, g)
 
     def prepare():
         for copy in small[2:]:
@@ -272,8 +269,7 @@
         return jnp.sum(jnp.where(diagonal, phase, 0.0), axis=1, keepdims=True)
 
     def mix(l, h):
-        for o in range(1, n_dp):
-            copies["sq", l, h, o].wait_recv()
+        arrived(sq_got.at[l, h], sq_recv.at[l, h])
         line = sq_sent[l, h]
         for o in range(1, n_dp):
             line = line + sq_got[l, h, o - 1]
@@ -281,8 +277,9 @@
         inv_rms = lax.rsqrt(squares / (depth * n_dp) + NORM_EPS)
 
         def total(c):
-            for o in range(1, n_dp):
-                copies["rs", l, h, c, o].wait_recv()
+            for g in range(len(GROUPS)):
+                if GROUPS[g][0] == c:
+                    arrived(got.at[l, h, :, :, columns_of(g)], rs_recv.at[l, h, g])
             cols = pl.ds(starts[c], sizes[c])
             out = sent[l, h, mine, cols].astype(F32)
             for o in range(1, n_dp):
@@ -340,13 +337,8 @@
             cols = slice(j * LANES, (j + 1) * LANES)
             mixed_all[l, h, mine, cols] = (jnp.where(low, even, odd) * gate[:, cols]).astype(BF16)
         for o in range(1, n_dp):
-            describe(
-                ("ag", l, h, o),
-                mixed_all.at[l, h, mine],
-                mixed_all.at[l, h, mine],
-                ag_send.at[l, h, o - 1],
-                ag_recv.at[l, h, o - 1],
-                {"dp": dp_peer(o)},
+            copy_of(
+                mixed_all.at[l, h, mine], mixed_all.at[l, h, mine], ag_send, ag_recv.at[l, h], {"dp": dp_peer(o)}
             ).start()
 
         def split(v):
@@ -371,8 +363,7 @@
         lax.fori_loop(first, last, one, 0, unroll=True)
 
     def output(l, h):
-        for o in range(1, n_dp):
-            copies["ag", l, h, o].wait_recv()
+        arrived(mixed_all.at[l, h, : (n_dp - 1) * own], ag_recv.at[l, h])
         if h == 0:
             loads[l, 6].wait()
         product = jnp.dot(mixed_all[l, h], wo[l], preferred_element_type=F32).astype(BF16)
@@ -382,13 +373,8 @@
                 i * part_rows : (i + 1) * part_rows, j * part_cols : (j + 1) * part_cols
             ]
         for k in range(reducers):
-            copy = describe(
-                ("tr", l, h, k),
-                terms.at[l, h, k],
-                terms_got.at[l, h, lane_me],
-                tr_send.at[l, h, k],
-                tr_recv.at[l, h, lane_me],
-                {"tp": first + k},
+            copy = copy_of(
+                terms.at[l, h, k], terms_got.at[l, h, lane_me], tr_send, tr_recv.at[l, h], {"tp": first + k}
             )
             pl.when(lane_me != first + k)(copy.start)
 
@@ -396,16 +382,6 @@
     slot = jnp.clip(lane_me - first, 0, reducers - 1)
 
     def gather_terms(l, h):
-        for o in range(1, n_tp):
-            describe(
-                ("ta", l, h, o),
-                fresh.at[l, h, slot],
-                fresh.at[l, h, slot],
-                ta_send.at[l, h, o - 1],
-                ta_recv.at[l, h, slot],
-                {"tp": tp_peer(o)},
-            )
-
         @pl.when(reducing)
         def _():
             acc = terms[l, h, slot].astype(F32)
@@ -415,32 +391,25 @@
                 acc = acc + x_ref[h, at_rows, at_cols].astype(F32)
             else:
                 acc = acc + fresh[l - 1, h, slot].astype(F32)
+            arrived(terms_got.at[l, h, : n_tp - 1], tr_recv.at[l, h])
             for o in range(1, n_tp):
-                there = tp_peer(o)
-                pltpu.make_async_remote_copy(
-                    src_ref=terms.at[l, h, slot],
-                    dst_ref=terms_got.at[l, h, there],
-                    send_sem=tr_send.at[l, h, slot],
-                    recv_sem=tr_recv.at[l, h, there],
-                    device_id={"tp": there},
-                    device_id_type=MESH,
-                ).wait_recv()
-                acc = acc + terms_got[l, h, there].astype(F32)
+                acc = acc + terms_got[l, h, tp_peer(o)].astype(F32)
             fresh[l, h, slot] = acc.astype(BF16)
             for o in range(1, n_tp):
-                copies["ta", l, h, o].start()
+                copy_of(
+                    fresh.at[l, h, slot], fresh.at[l, h, slot], ta_send, ta_recv.at[l, h], {"tp": tp_peer(o)}
+                ).start()
 
     def renew(l, h):
-        for k in range(reducers):
-            copy = pltpu.make_async_remote_copy(
-                src_ref=fresh.at[l, h, k],
-                dst_ref=fresh.at[l, h, k],
-                send_sem=ta_send.at[l, h, 0],
-                recv_sem=ta_recv.at[l, h, k],
-                device_id={"tp": tp_peer(1)},
-                device_id_type=MESH,
-            )
-            pl.when(lane_me != first + k)(copy.wait_recv)
+        @pl.when(reducing)
+        def _():
+            arrived(fresh.at[l, h, : reducers - 1], ta_recv.at[l, h])
+
+        if reducers < n_tp:
+
+            @pl.when(jnp.logical_not(reducing))
+            def _():
+                arrived(fresh.at[l, h], ta_recv.at[l, h])
 
     def finish(h):
         for i in range(reducers // strips):
@@ -478,17 +447,20 @@
     for h in every:
         renew(BLOCK_COUNT - 1, h)
         finish(h)
-    for key, copy in copies.items():
-        if key[0] == "tr":
-            pl.when(lane_me != first + key[3])(copy.wait_send)
-        elif key[0] != "ta":
-            copy.wait_send()
+    left(got, rs_send)
+    left(sq_got, sq_send)
+    left(mixed_all.at[:, :, : (n_dp - 1) * own], ag_send)
 
     @pl.when(reducing)
     def _():
-        for key, copy in copies.items():
-            if key[0] == "ta":
-                copy.wait_send()
+        left(terms.at[:, :, : reducers - 1], tr_send)
+        left(terms_got.at[:, :, : n_tp - 1], ta_send)
+
+    if reducers < n_tp:
+
+        @pl.when(jnp.logical_not(reducing))
+        def _():
+            left(terms, tr_send)
 
 
 def flush(out, state, out_hbm, state_hbm, sem):
@@ -579,16 +551,16 @@
                 pltpu.VMEM((LANES, vk), BF16),
                 dma((7,)),
                 dma((blocks, 7)),
-                dma((blocks, halves, 5, n_dp - 1)),
-                dma((blocks, halves, 5, n_dp - 1)),
-                dma((blocks, halves, n_dp - 1)),
-                dma((blocks, halves, n_dp - 1)),
-                dma((blocks, halves, n_dp - 1)),
-                dma((blocks, halves, n_dp - 1)),
-                dma((blocks, halves, reducers)),
-                dma((blocks, halves, n_tp)),
-                dma((blocks, halves, n_tp - 1)),
-                dma((blocks, halves, reducers)),
+                dma,
+                dma((blocks, halves, len(GROUPS))),
+                dma,
+                dma((blocks, halves)),
+                dma,
+                dma((blocks, halves)),
+                dma,
+                dma((blocks, halves)),
+                dma,
+                dma((blocks, halves)),
             ],
             compiler_params=pltpu.CompilerParams(
                 collective_id=0, has_side_effects=True, vmem_limit_bytes=54 * 1024 * 1024

time: 54.9 us -> 52.8 us (0.962)
  Pallas kernels: 54.2 us -> 52 us
    pallas_call x1, Pallas kernels: 50.7 us -> 48.5 us  [body(): pl.pallas_call(functools.partial(kernel, n_dp, n_tp, halves), out_shape=(...]
where the time goes in v3:
time: 52.8 us; the launch traced here: 52.6 us
  Pallas kernels  52 us (98%)
  between operations  0.64 us (1%)
    pallas_call x1, Pallas kernels, body(): pl.pallas_call(functools.partial(kernel, n_dp, n_tp, halves), out_shape=(...  48.5 us
    pallas_call x1, Pallas kernels, body(): pl.pallas_call(flush, out_shape=(jax.ShapeDtypeStruct((batch, depth), BF1...  3.46 us

profile of v3, /device:TPU:0, one launch (start us, length us, event | category | flops | bytes accessed | tf_op | source)
XLA Modules:
  0.0 52.6 jit_solution(1001959015182641204)
XLA Ops:
  0.6 48.5 %shard_map.149 = (bf16[128,1024]{1,0:T(8,128)(2,1)S(1)}, f32[2,256,4096]{2,1,0:T(8,128)S(1)}) custom-call(bf16[128,1024]{1,0:T(8,128)(2,1)} %stream_hbm.1, s32[1,32]{1,0:T(1,128)} %bitcast.4, f32[2,1024]{1,0:T(2,128)} %in_gain_hbm.1, bf16[2,1024,128]{2,1,0:T(8,128)(2,1)} %adapter_hbm.1, bf16[2,1024,512]{2,1,0:T(8,128)(2,1)} %key_hbm.1, ...), custom_call_target="tpu_custom_call" | custom-call | tf_op jit(solution)/shard_map/pallas_call | solution.py:516
  49.2 3.5 %shard_map.150 = (bf16[128,1024]{1,0:T(8,128)(2,1)}, f32[2,256,4096]{2,1,0:T(8,128)}) custom-call(bf16[128,1024]{1,0:T(8,128)(2,1)S(1)} %get-tuple-element.6.out, f32[2,256,4096]{2,1,0:T(8,128)S(1)} %get-tuple-element.7.state), custom_call_target="tpu_custom_call" | custom-call | tf_op jit(solution)/shard_map/pallas_call | solution.py:584

commit v4 on v3

--- a/solution.py
+++ b/solution.py
@@ -362,6 +362,12 @@
 
         lax.fori_loop(first, last, one, 0, unroll=True)
 
+    def far_first(i):
+        begin = jnp.where(lane_me < n_tp // 2, reducers // 2, 0)
+        odd = lax.rem(lane_me, 2)
+        turn = odd * (1 - 2 * (i % 2))
+        return lax.rem(begin + i + turn + reducers, reducers)
+
     def output(l, h):
         arrived(mixed_all.at[l, h, : (n_dp - 1) * own], ag_recv.at[l, h])
         if h == 0:
@@ -372,7 +378,8 @@
             terms[l, h, k] = product[
                 i * part_rows : (i + 1) * part_rows, j * part_cols : (j + 1) * part_cols
             ]
-        for k in range(reducers):
+        for i in range(reducers):
+            k = far_first(i)
             copy = copy_of(
                 terms.at[l, h, k], terms_got.at[l, h, lane_me], tr_send, tr_recv.at[l, h], {"tp": first + k}
             )

time: 52.8 us -> 52.3 us (level)
  no operation moved by 1% of the time
where the time goes in v4:
time: 52.3 us; the launch traced here: 52.2 us
  Pallas kernels  51.5 us (98%)
  between operations  0.64 us (1%)
    pallas_call x1, Pallas kernels, body(): pl.pallas_call(functools.partial(kernel, n_dp, n_tp, halves), out_shape=(...  48 us
    pallas_call x1, Pallas kernels, body(): pl.pallas_call(flush, out_shape=(jax.ShapeDtypeStruct((batch, depth), BF1...  3.46 us

profile of v4, /device:TPU:0, one launch (start us, length us, event | category | flops | bytes accessed | tf_op | source)
XLA Modules:
  0.0 52.2 jit_solution(10661109537084569186)
XLA Ops:
  0.6 48.0 %shard_map.149 = (bf16[128,1024]{1,0:T(8,128)(2,1)S(1)}, f32[2,256,4096]{2,1,0:T(8,128)S(1)}) custom-call(bf16[128,1024]{1,0:T(8,128)(2,1)} %stream_hbm.1, s32[1,32]{1,0:T(1,128)} %bitcast.4, f32[2,1024]{1,0:T(2,128)} %in_gain_hbm.1, bf16[2,1024,128]{2,1,0:T(8,128)(2,1)} %adapter_hbm.1, bf16[2,1024,512]{2,1,0:T(8,128)(2,1)} %key_hbm.1, ...), custom_call_target="tpu_custom_call" | custom-call | tf_op jit(solution)/shard_map/pallas_call | solution.py:523
  48.7 3.5 %shard_map.150 = (bf16[128,1024]{1,0:T(8,128)(2,1)}, f32[2,256,4096]{2,1,0:T(8,128)}) custom-call(bf16[128,1024]{1,0:T(8,128)(2,1)S(1)} %get-tuple-element.6.out, f32[2,256,4096]{2,1,0:T(8,128)S(1)} %get-tuple-element.7.state), custom_call_target="tpu_custom_call" | custom-call | tf_op jit(solution)/shard_map/pallas_call | solution.py:591

commit v5 on v4

--- a/solution.py
+++ b/solution.py
@@ -17,7 +17,7 @@
 TILE = 256
 FLUSHES = 8
 PIECES = 2
-GROUPS = ((0,), (1,), (2,), (3,), (4,))
+GROUPS = ((0, 1), (2,), (3, 4))
 MESH = pl.DeviceIdType.MESH
 F32 = jnp.float32
 BF16 = jnp.bfloat16
@@ -194,11 +194,11 @@
         copy_of(ref, ref, tr_send, recv, {"tp": tp_peer(1)}).wait_recv()
 
     def left(ref, send):
-        copy_of(ref, ref, send, ta_recv.at[0, 0], {"tp": tp_peer(1)}).wait_send()
+        copy_of(ref, ref, send, ta_recv.at[0], {"tp": tp_peer(1)}).wait_send()
 
     def send_squares(l, h):
         for o in range(1, n_dp):
-            copy_of(sq_sent.at[l, h], sq_got.at[l, h, o - 1], sq_send, sq_recv.at[l, h], {"dp": dp_peer(o)}).start()
+            copy_of(sq_sent.at[l, h], sq_got.at[l, h, o - 1], sq_send, sq_recv.at[h], {"dp": dp_peer(o)}).start()
 
     def columns_of(g):
         return pl.ds(starts[GROUPS[g][0]], sum(sizes[c] for c in GROUPS[g]))
@@ -209,7 +209,7 @@
             there = dp_peer(o)
             at = pl.ds(pl.multiple_of(there * own, own), own)
             copy_of(
-                sent.at[l, h, at, cols], got.at[l, h, o - 1, :, cols], rs_send, rs_recv.at[l, h, g], {"dp": there}
+                sent.at[l, h, at, cols], got.at[l, h, o - 1, :, cols], rs_send, rs_recv.at[h, g], {"dp": there}
             ).start()
 
     def put_squares(l, h, x):
@@ -269,7 +269,7 @@
         return jnp.sum(jnp.where(diagonal, phase, 0.0), axis=1, keepdims=True)
 
     def mix(l, h):
-        arrived(sq_got.at[l, h], sq_recv.at[l, h])
+        arrived(sq_got.at[l, h], sq_recv.at[h])
         line = sq_sent[l, h]
         for o in range(1, n_dp):
             line = line + sq_got[l, h, o - 1]
@@ -279,7 +279,7 @@
         def total(c):
             for g in range(len(GROUPS)):
                 if GROUPS[g][0] == c:
-                    arrived(got.at[l, h, :, :, columns_of(g)], rs_recv.at[l, h, g])
+                    arrived(got.at[l, h, :, :, columns_of(g)], rs_recv.at[h, g])
             cols = pl.ds(starts[c], sizes[c])
             out = sent[l, h, mine, cols].astype(F32)
             for o in range(1, n_dp):
@@ -338,7 +338,7 @@
             mixed_all[l, h, mine, cols] = (jnp.where(low, even, odd) * gate[:, cols]).astype(BF16)
         for o in range(1, n_dp):
             copy_of(
-                mixed_all.at[l, h, mine], mixed_all.at[l, h, mine], ag_send, ag_recv.at[l, h], {"dp": dp_peer(o)}
+                mixed_all.at[l, h, mine], mixed_all.at[l, h, mine], ag_send, ag_recv.at[h], {"dp": dp_peer(o)}
             ).start()
 
         def split(v):
@@ -369,7 +369,7 @@
         return lax.rem(begin + i + turn + reducers, reducers)
 
     def output(l, h):
-        arrived(mixed_all.at[l, h, : (n_dp - 1) * own], ag_recv.at[l, h])
+        arrived(mixed_all.at[l, h, : (n_dp - 1) * own], ag_recv.at[h])
         if h == 0:
             loads[l, 6].wait()
         product = jnp.dot(mixed_all[l, h], wo[l], preferred_element_type=F32).astype(BF16)
@@ -381,7 +381,7 @@
         for i in range(reducers):
             k = far_first(i)
             copy = copy_of(
-                terms.at[l, h, k], terms_got.at[l, h, lane_me], tr_send, tr_recv.at[l, h], {"tp": first + k}
+                terms.at[l, h, k], terms_got.at[l, h, lane_me], tr_send, tr_recv.at[h], {"tp": first + k}
             )
             pl.when(lane_me != first + k)(copy.start)
 
@@ -398,25 +398,25 @@
                 acc = acc + x_ref[h, at_rows, at_cols].astype(F32)
             else:
                 acc = acc + fresh[l - 1, h, slot].astype(F32)
-            arrived(terms_got.at[l, h, : n_tp - 1], tr_recv.at[l, h])
+            arrived(terms_got.at[l, h, : n_tp - 1], tr_recv.at[h])
             for o in range(1, n_tp):
                 acc = acc + terms_got[l, h, tp_peer(o)].astype(F32)
             fresh[l, h, slot] = acc.astype(BF16)
             for o in range(1, n_tp):
                 copy_of(
-                    fresh.at[l, h, slot], fresh.at[l, h, slot], ta_send, ta_recv.at[l, h], {"tp": tp_peer(o)}
+                    fresh.at[l, h, slot], fresh.at[l, h, slot], ta_send, ta_recv.at[h], {"tp": tp_peer(o)}
                 ).start()
 
     def renew(l, h):
         @pl.when(reducing)
         def _():
-            arrived(fresh.at[l, h, : reducers - 1], ta_recv.at[l, h])
+            arrived(fresh.at[l, h, : reducers - 1], ta_recv.at[h])
 
         if reducers < n_tp:
 
             @pl.when(jnp.logical_not(reducing))
             def _():
-                arrived(fresh.at[l, h], ta_recv.at[l, h])
+                arrived(fresh.at[l, h], ta_recv.at[h])
 
     def finish(h):
         for i in range(reducers // strips):
@@ -559,15 +559,15 @@
                 dma((7,)),
                 dma((blocks, 7)),
                 dma,
-                dma((blocks, halves, len(GROUPS))),
+                dma((halves, len(GROUPS))),
                 dma,
-                dma((blocks, halves)),
+                dma((halves,)),
                 dma,
-                dma((blocks, halves)),
+                dma((halves,)),
                 dma,
-                dma((blocks, halves)),
+                dma((halves,)),
                 dma,
-                dma((blocks, halves)),
+                dma((halves,)),
             ],
             compiler_params=pltpu.CompilerParams(
                 collective_id=0, has_side_effects=True, vmem_limit_bytes=54 * 1024 * 1024

time: 52.3 us -> 52.1 us (level)
  no operation moved by 1% of the time
where the time goes in v5:
time: 52.1 us; the launch traced here: 51.9 us
  Pallas kernels  51.3 us (98%)
  between operations  0.64 us (1%)
    pallas_call x1, Pallas kernels, body(): pl.pallas_call(functools.partial(kernel, n_dp, n_tp, halves), out_shape=(...  47.8 us
    pallas_call x1, Pallas kernels, body(): pl.pallas_call(flush, out_shape=(jax.ShapeDtypeStruct((batch, depth), BF1...  3.46 us

profile of v5, /device:TPU:0, one launch (start us, length us, event | category | flops | bytes accessed | tf_op | source)
XLA Modules:
  0.0 51.9 jit_solution(12356757376813742153)
XLA Ops:
  0.6 47.8 %shard_map.149 = (bf16[128,1024]{1,0:T(8,128)(2,1)S(1)}, f32[2,256,4096]{2,1,0:T(8,128)S(1)}) custom-call(bf16[128,1024]{1,0:T(8,128)(2,1)} %stream_hbm.1, s32[1,32]{1,0:T(1,128)} %bitcast.4, f32[2,1024]{1,0:T(2,128)} %in_gain_hbm.1, bf16[2,1024,128]{2,1,0:T(8,128)(2,1)} %adapter_hbm.1, bf16[2,1024,512]{2,1,0:T(8,128)(2,1)} %key_hbm.1, ...), custom_call_target="tpu_custom_call" | custom-call | tf_op jit(solution)/shard_map/pallas_call | solution.py:523
  48.5 3.5 %shard_map.150 = (bf16[128,1024]{1,0:T(8,128)(2,1)}, f32[2,256,4096]{2,1,0:T(8,128)}) custom-call(bf16[128,1024]{1,0:T(8,128)(2,1)S(1)} %get-tuple-element.6.out, f32[2,256,4096]{2,1,0:T(8,128)S(1)} %get-tuple-element.7.state), custom_call_target="tpu_custom_call" | custom-call | tf_op jit(solution)/shard_map/pallas_call | solution.py:591
